TPU v7x, 32 devices: a whole 2x2x4 slice. The times are simulated.
32 devices in a mesh: ep: 16 (over z, y, x), tp: 2 (over core).
Axes of the slice: x: 2, y: 2, z: 4, core: 2. Of those that a mesh axis runs over, the one named last changes fastest.
Arguments:
- hidden_in: bfloat16 [512, 2048], P('ep'), may hold values from -6 to 6
- past_lengths: int32 [512], P('ep'), may hold values from 1 to 1023, as said below
- key_cache: bfloat16 [512, 1024, 256], P('ep', None, 'tp'), may hold values from -512 to 512
- value_cache: bfloat16 [512, 1024, 256], P('ep', None, 'tp'), may hold values from -6 to 6
- attn_gain: float32 [2048], replicated, may hold values from 0.1 to 1.9
- w_query: bfloat16 [2048, 2048], P(None, 'tp'), may hold values from -0.125 to 0.125
- w_key: bfloat16 [2048, 256], P(None, 'tp'), may hold values from -0.125 to 0.125
- w_value: bfloat16 [2048, 256], P(None, 'tp'), may hold values from -0.125 to 0.125
- lambdas: float32 [16], P('tp'), may hold values from 0.3 to 0.8
- head_gain: float32 [128], replicated, may hold values from 0.1 to 1.9
- w_out: bfloat16 [2048, 2048], P('tp'), may hold values from -0.125 to 0.125
- ffn_gain: float32 [2048], replicated, may hold values from 0.1 to 1.9
- route_ids: int32 [512, 2], P('ep'), may hold values from 0 to 7, all different within a row; in each aligned block of 32 rows (0 to 31, 32 to 63, ...) at most 16 rows name the same one
- route_weights: float32 [512, 2], P('ep'), may hold values from 0.2 to 1
- expert_gate: bfloat16 [16, 2048, 704], P('ep', None, 'tp'), may hold values from -0.125 to 0.125
- expert_up: bfloat16 [16, 2048, 704], P('ep', None, 'tp'), may hold values from -0.125 to 0.125
- expert_down: bfloat16 [16, 704, 2048], P('ep', None, 'tp'), may hold values from -1.25 to 1.25
- gate_vector: bfloat16 [2048], replicated, may hold values from -0.125 to 0.125
- dense_gate: bfloat16 [2048, 5632], P(None, ('ep', 'tp')), may hold values from -0.125 to 0.125
- dense_up: bfloat16 [2048, 5632], P(None, ('ep', 'tp')), may hold values from -0.125 to 0.125
- dense_down: bfloat16 [5632, 2048], P('ep', 'tp'), may hold values from -0.625 to 0.625
Outputs:
- mixed_out: bfloat16 [512, 2048], P('ep', 'tp')
- new_keys: bfloat16 [512, 256], P('ep', 'tp')
- new_values: bfloat16 [512, 256], P('ep', 'tp')
Inputs may be any that keep to these rules, and one draw needn't show every extreme that they name: `past_lengths`: the new token of a sequence stands at this position; some sequence has 1023 cached positions in every draw. `route_ids`: each row names 2 different experts; among the rows of one index of ep no expert is named more than 16 times, a bound that some block reaches in every draw.
All inputs are finite; a program needn't handle non-finite values.
Results may differ from a plain program's by a relative error of at most 0.02.
The roundings to bfloat16 on the way count: a program that leaves them out, or rounds other values in their place, can miss the bound.
Values may be sent and summed in bfloat16 or wider, within the bound.
A program may use at most 128 MiB of HBM per device.

v0:
```python
import jax
import jax.numpy as jnp
from jax import lax
from jax.sharding import PartitionSpec as P

HEAD_DIM = 64
VALUE_DIM = 128


norm_eps = 1e-05
rope_base = 10000.0


def rms_rows(values, scales):
    values = values.astype(jnp.float32)
    return values * lax.rsqrt(jnp.mean(values * values, axis=-1, keepdims=True) + norm_eps) * scales


def rotary(values, position):
    middle = values.shape[-1] // 2
    inverse = rope_base ** (-jnp.arange(middle, dtype=jnp.float32) / middle)
    angles = position.astype(jnp.float32)[:, None] * inverse[None, :]
    cosine = jnp.cos(angles)[:, None, None, :]
    sine_part = jnp.sin(angles)[:, None, None, :]
    leading, second = (values[..., :middle], values[..., middle:])
    return jnp.concatenate(
        [leading * cosine - second * sine_part, second * cosine + leading * sine_part], axis=-1
    )


def per_device(
    hidden_in,
    past_lengths,
    key_cache,
    value_cache,
    attn_gain,
    w_query,
    w_key,
    w_value,
    lambdas,
    head_gain,
    w_out,
    ffn_gain,
    route_ids,
    route_weights,
    expert_gate,
    expert_up,
    expert_down,
    gate_vector,
    dense_gate,
    dense_up,
    dense_down,
):
    batch_rows = hidden_in.shape[0]
    model_width = hidden_in.shape[1]
    tp_count = lax.axis_size("tp")
    ep_count = lax.axis_size("ep")
    tp_rank = lax.axis_index("tp")
    half_width = model_width // tp_count
    heads_here = lambdas.shape[0]
    kv_here = w_key.shape[1] // (2 * HEAD_DIM)
    per_key = heads_here // kv_here
    scale_qk = HEAD_DIM ** (-0.5)
    normed = rms_rows(hidden_in, attn_gain).astype(jnp.bfloat16)
    queries = rotary(
        jnp.dot(normed, w_query, preferred_element_type=jnp.float32).reshape(
            batch_rows, heads_here, 2, HEAD_DIM
        ),
        past_lengths,
    ).astype(jnp.bfloat16)
    key_new = rotary(
        jnp.dot(normed, w_key, preferred_element_type=jnp.float32).reshape(
            batch_rows, kv_here, 2, HEAD_DIM
        ),
        past_lengths,
    ).astype(jnp.bfloat16)
    value_new = jnp.dot(normed, w_value, preferred_element_type=jnp.float32).astype(jnp.bfloat16)
    grouped = queries.reshape(batch_rows, kv_here, per_key, 2, HEAD_DIM)
    own_score = (
        jnp.einsum("sgamd,sgmd->sgam", grouped, key_new, preferred_element_type=jnp.float32)
        * scale_qk
    )
    value_rows = value_new.reshape(batch_rows, kv_here, 1, 1, VALUE_DIM).astype(jnp.float32)
    start_state = (
        own_score,
        jnp.ones_like(own_score),
        jnp.broadcast_to(value_rows, own_score.shape + (VALUE_DIM,)),
    )
    cache_len = key_cache.shape[1]
    span_len = min(256, cache_len)
    spans_needed = (jnp.max(past_lengths) + span_len - 1) // span_len

    def visit(block_index, carried):
        running, totals, summed = carried
        offset = block_index * span_len
        key_rows = lax.dynamic_slice_in_dim(key_cache, offset, span_len, 1).reshape(
            batch_rows, span_len, kv_here, 2, HEAD_DIM
        )
        cached = lax.dynamic_slice_in_dim(value_cache, offset, span_len, 1).reshape(
            batch_rows, span_len, kv_here, VALUE_DIM
        )
        scores = (
            jnp.einsum("sgamd,slgmd->sgaml", grouped, key_rows, preferred_element_type=jnp.float32)
            * scale_qk
        )
        usable = (offset + jnp.arange(span_len))[None, :] < past_lengths[:, None]
        scores = jnp.where(usable[:, None, None, None, :], scores, -jnp.inf)
        raised = jnp.maximum(running, jnp.max(scores, axis=-1))
        fading = jnp.exp(running - raised)
        weights = jnp.exp(scores - raised[..., None])
        totals = totals * fading + jnp.sum(weights, axis=-1)
        summed = summed * fading[..., None] + jnp.einsum(
            "sgaml,slge->sgame",
            weights.astype(jnp.bfloat16),
            cached,
            preferred_element_type=jnp.float32,
        )
        return (raised, totals, summed)

    running, totals, summed = lax.fori_loop(0, spans_needed, visit, start_state)
    mapped = summed / totals[..., None]
    head_mix = mapped[..., 0, :] - lambdas.reshape(1, kv_here, per_key, 1) * mapped[..., 1, :]
    head_out = rms_rows(head_mix, head_gain).astype(jnp.bfloat16).reshape(batch_rows, -1)
    attn_out = lax.psum(
        jnp.dot(head_out, w_out, preferred_element_type=jnp.float32).astype(jnp.bfloat16), "tp"
    )
    residual = hidden_in.astype(jnp.float32) + attn_out.astype(jnp.float32)
    moe_in = rms_rows(residual, ffn_gain).astype(jnp.bfloat16)
    mix_gate = jax.nn.sigmoid(
        jnp.dot(moe_in, gate_vector, preferred_element_type=jnp.float32)
    ).astype(jnp.bfloat16)
    top_count = route_ids.shape[1]
    experts = ep_count // 2
    capacity = max(2, 2 * batch_rows * top_count // experts)
    flat_ids = route_ids.reshape(-1)
    matches = (flat_ids[:, None] == jnp.arange(experts)[None, :]).astype(jnp.int32)
    earlier = jnp.sum((jnp.cumsum(matches, axis=0) - matches) * matches, axis=1)
    slot_of = flat_ids * capacity + earlier
    placing = (jnp.arange(experts * capacity)[:, None] == slot_of[None, :]).astype(jnp.float32)
    repeated = jnp.repeat(moe_in, top_count, axis=0)
    packed = jnp.dot(
        placing.astype(jnp.bfloat16), repeated, preferred_element_type=jnp.float32
    ).astype(jnp.bfloat16)
    outgoing = jnp.broadcast_to(
        packed.reshape(experts, 1, capacity, model_width), (experts, 2, capacity, model_width)
    ).reshape(ep_count, capacity, model_width)
    arrived = lax.all_to_all(outgoing, "ep", split_axis=0, concat_axis=0, tiled=True)
    leading = arrived.shape[:2]
    flat_rows = arrived.reshape(-1, model_width)
    gate_pre = jnp.dot(flat_rows, expert_gate[0], preferred_element_type=jnp.float32)
    up_pre = jnp.dot(flat_rows, expert_up[0], preferred_element_type=jnp.float32)
    inner_act = (jax.nn.silu(gate_pre) * up_pre).astype(jnp.bfloat16)
    inner_act = lax.all_gather(inner_act, "tp", axis=1, tiled=True)
    partial_value = jnp.dot(inner_act, expert_down[0], preferred_element_type=jnp.float32).reshape(
        leading + (half_width,)
    )
    returned = lax.all_to_all(
        partial_value.astype(jnp.bfloat16), "ep", split_axis=0, concat_axis=0, tiled=True
    ).astype(partial_value.dtype)
    paired = jnp.sum(returned.reshape(experts, 2, capacity, half_width), axis=1).reshape(
        experts * capacity, half_width
    )
    weighted = (
        (placing * route_weights.reshape(1, -1))
        .reshape(experts * capacity, batch_rows, top_count)
        .sum(axis=2)
    )
    moe_out = jnp.einsum("ct,cd->td", weighted, paired, precision=lax.Precision.HIGHEST)
    rows_all, gates_all = (
        lax.all_gather(moe_in, "ep", axis=0, tiled=True),
        lax.all_gather(mix_gate, "ep", axis=0, tiled=True),
    )
    local_pre = jnp.dot(rows_all, dense_gate, preferred_element_type=jnp.float32)
    local_up = jnp.dot(rows_all, dense_up, preferred_element_type=jnp.float32)
    local_act = (jax.nn.silu(local_pre) * local_up).astype(jnp.bfloat16)
    dense_act = lax.all_gather(local_act, "tp", axis=1, tiled=True)
    gate_rows = gates_all.astype(jnp.float32)
    dense_out = lax.psum_scatter(
        jnp.dot(dense_act, dense_down, preferred_element_type=jnp.float32) * gate_rows[:, None],
        "ep",
        scatter_dimension=0,
        tiled=True,
    )
    own_residual = lax.dynamic_slice_in_dim(residual, tp_rank * half_width, half_width, 1)
    mixed_out = (own_residual + moe_out + dense_out).astype(jnp.bfloat16)
    return (mixed_out, key_new.reshape(batch_rows, -1), value_new)


def solution(mesh):
    return jax.shard_map(
        per_device,
        mesh=mesh,
        in_specs=(
            P("ep", None),
            P("ep"),
            P("ep", None, "tp"),
            P("ep", None, "tp"),
            P(),
            P(None, "tp"),
            P(None, "tp"),
            P(None, "tp"),
            P("tp"),
            P(),
            P("tp", None),
            P(),
            P("ep", None),
            P("ep", None),
            P("ep", None, "tp"),
            P("ep", None, "tp"),
            P("ep", None, "tp"),
            P(),
            P(None, ("ep", "tp")),
            P(None, ("ep", "tp")),
            P("ep", "tp"),
        ),
        out_specs=(P("ep", "tp"), P("ep", "tp"), P("ep", "tp")),
        check_vma=False,
    )
```

profile of v0, /device:TPU:0, one launch (start us, length us, event | category | flops | bytes accessed | tf_op | source)
XLA Modules:
  0.0 262.9 jit_solution(17510185976092909314)
XLA Ops:
  7.2 1.4 fusion.67
  10.4 1.4 fusion.62
  11.9 3.2 %fusion.60 = f32[32,1024]{1,0:T(8,128)S(1)} fusion(bf16[2048,1024]{1,0:T(8,128)(2,1)} %param.28, bf16[32,2048]{1,0:T(8,128)(2,1)} %param.23, f32[2048]{0:T(1024)} %param.27, f32[32]{0:T(128)S(1)} %add_rsqrt_fusion.2), kind=kOutput, calls=%fused_computation.98 | convolution fusion | flops 134479872 | bytes 4464768 | tf_op jit(solution)/shard_map/dot_general | solution.py:66
  19.8 36.4 %while.14 = (s32[]{:T(128)}, f32[32,1,8,2]{2,3,0,1:T(2,128)}, f32[32,1,8,2]{2,3,0,1:T(2,128)}, f32[32,1,8,2,128]{4,2,3,0,1:T(8,128)}, s32[]{:T(128)}, /*index=5*...) while((s32[]{:T(128)}, f32[32,1,8,2]{2,3,0,1:T(2,128)}, ...), condition=%wide.region_5.6_spmd, body=%wide.region_2.5_spmd.sunk | while | flops 51390212 | bytes 16918980 | solution.py:120
  19.8 3.2 %constant_dynamic-slice_fusion.2 = bf16[32,256,128]{2,1,0:T(8,128)(2,1)} fusion(bf16[32,1024,128]{2,1,0:T(8,128)(2,1)} %get-tuple-element.224, s32[]{:T(128)S(6)} %select_n.25), kind=kLoop, calls=%fused_computation.22.clone.1 | loop fusion | bytes 4194308 | tf_op jit(solution)/shard_map/while/body/dynamic_slice | solution.py:96
  23.0 3.3 %copy.81 = bf16[32,256,128]{1,2,0:T(8,128)(2,1)S(1)} copy(bf16[32,256,128]{2,1,0:T(8,128)(2,1)} %constant_dynamic-slice_fusion.2) | data formatting | bytes 4194304 | tf_op jit(solution)/shard_map/while/body/dynamic_slice | solution.py:96
  27.1 1.4 fusion.98
  28.5 2.1 fusion.101
  32.0 3.2 %constant_dynamic-slice_fusion.2 = bf16[32,256,128]{2,1,0:T(8,128)(2,1)} fusion(bf16[32,1024,128]{2,1,0:T(8,128)(2,1)} %get-tuple-element.224, s32[]{:T(128)S(6)} %select_n.25), kind=kLoop, calls=%fused_computation.22.clone.1 | loop fusion | bytes 4194308 | tf_op jit(solution)/shard_map/while/body/dynamic_slice | solution.py:96
  35.1 3.3 %copy.81 = bf16[32,256,128]{1,2,0:T(8,128)(2,1)S(1)} copy(bf16[32,256,128]{2,1,0:T(8,128)(2,1)} %constant_dynamic-slice_fusion.2) | data formatting | bytes 4194304 | tf_op jit(solution)/shard_map/while/body/dynamic_slice | solution.py:96
  39.2 1.4 fusion.98
  40.7 2.1 fusion.101
  44.1 3.2 %constant_dynamic-slice_fusion.2 = bf16[32,256,128]{2,1,0:T(8,128)(2,1)} fusion(bf16[32,1024,128]{2,1,0:T(8,128)(2,1)} %get-tuple-element.224, s32[]{:T(128)S(6)} %select_n.25), kind=kLoop, calls=%fused_computation.22.clone.1 | loop fusion | bytes 4194308 | tf_op jit(solution)/shard_map/while/body/dynamic_slice | solution.py:96
  47.3 3.3 %copy.81 = bf16[32,256,128]{1,2,0:T(8,128)(2,1)S(1)} copy(bf16[32,256,128]{2,1,0:T(8,128)(2,1)} %constant_dynamic-slice_fusion.2) | data formatting | bytes 4194304 | tf_op jit(solution)/shard_map/while/body/dynamic_slice | solution.py:96
  51.3 1.4 fusion.98
  52.8 2.1 fusion.101
  56.2 1.1 broadcast_divide_fusion
  59.1 3.7 %convolution_convert_fusion.1 = bf16[32,2048]{1,0:T(8,128)(2,1)} fusion(bf16[1024,2048]{1,0:T(8,128)(2,1)} %param.33, f32[4,8,8,128]{3,2,1,0:T(8,128)S(1)} %bitcast.178, f32[4,8,8,128]{3,2,1,0:T(8,128)S(1)} %bitcast.180, f32[4,8,8,128]{3,2,1,0:T(8,128)S(1)} %bitcast.179, f32[1024]{0:T(1024)S(1)} %get-tuple-element.126, f32[1024]{0:T(1024)S(1)} %get-tuple-element.127), kind=kOutput, calls=%fused_computation.24 | convolution fusion | flops 134447104 | bytes 4726784 | tf_op jit(solution)/shard_map/dot_general | solution.py:125
  62.9 32.9 %all-reduce.3.cloned.1.call-done = bf16[32,2048]{1,0:T(8,128)(2,1)} async-done(((bf16[32,2048]{1,0:T(8,128)(2,1)}), bf16[32,2048]{1,0:T(8,128)(2,1)}) %all-reduce.3.cloned.1.call-update) | async-done | bytes 131088 | tf_op jit(solution)/shard_map/psum | solution.py:124
  96.9 1.6 multiply_convert_fusion
  102.9 42.2 %all-reduce = bf16[512]{0:T(512)(128)(2,1)S(1)} all-reduce(bf16[512]{0:T(512)(128)(2,1)S(1)} %dynamic-update-slice), channel_id=1, replica_groups=mesh['ep'=16,'tp'=2] {'ep'}, use_global_device_ids=true, to_apply=%add | all-reduce | flops 512 | bytes 2048
  145.1 15.5 %all-gather.2.cloned.1.call-done = bf16[512,2048]{1,0:T(8,128)(2,1)} async-done(((bf16[32,2048]{1,0:T(8,128)(2,1)}), bf16[512,2048]{1,0:T(8,128)(2,1)}) %all-gather.2.cloned.1.call-update) | async-done | bytes 2097168 | tf_op jit(solution)/shard_map/all_gather | solution.py:170
  160.6 2.6 fusion.68
  164.1 2.1 all_gather.14
  166.2 2.1 convolution_multiply_fusion.1
  168.7 38.9 %all_to_all.10 = bf16[16,16,2048]{2,1,0:T(8,128)(2,1)S(1)} all-to-all(bf16[16,16,2048]{2,1,0:T(8,128)(2,1)S(1)} %bitcast.170), channel_id=1, replica_groups=mesh['ep'=16,'tp'=2] {'ep'}, dimensions={0} | all-to-all | bytes 2097152 | tf_op jit(solution)/shard_map/all_to_all | solution.py:147
  208.8 2.1 all_gather.12
  211.0 1.4 fusion.26
  212.4 4.3 %all-to-all-start.1 = ((bf16[16,16,1024]{2,1,0:T(8,128)(2,1)}), bf16[16,16,1024]{2,1,0:T(8,128)(2,1)S(1)}, u32[]{:S(2)}, u32[]{:S(2)}) async-start(bf16[16,16,1024]{2,1,0:T(8,128)(2,1)} %fusion.26), calls=%async_computation.1 | async-start | bytes 1048576 | tf_op jit(solution)/shard_map/all_to_all | solution.py:157
  217.8 18.3 %all-to-all-done.1 = bf16[16,16,1024]{2,1,0:T(8,128)(2,1)S(1)} async-done(((bf16[16,16,1024]{2,1,0:T(8,128)(2,1)}), bf16[16,16,1024]{2,1,0:T(8,128)(2,1)S(1)}, u32[]{:S(2)}, u32[]{:S(2)}) %all-to-all-start.1) | async-done | bytes 524320 | tf_op jit(solution)/shard_map/all_to_all | solution.py:157
  236.2 18.2 %reduce-scatter.2.cloned.1.call-done = f32[32,1024]{1,0:T(8,128)} async-done(((f32[512,1024]{1,0:T(8,128)}), f32[32,1024]{1,0:T(8,128)}) %reduce-scatter.2.cloned.1.call-update) | async-done | bytes 131088 | tf_op jit(solution)/shard_map/reduce_scatter | solution.py:178
  254.4 1.9 fusion.37
  (142 shorter events, 22.6 us)
Async XLA Ops:
  7.2 203.8 %copy-start = (bf16[1,704,1024]{2,1,0:T(8,128)(2,1)S(1)}, bf16[1,704,1024]{2,1,0:T(8,128)(2,1)}, u32[]{:S(2)}) copy-start(bf16[1,704,1024]{2,1,0:T(8,128)(2,1)} %param.39) | copy-start | bytes 4325380
  7.2 88.6 %all-reduce.3.cloned.1.call-start = ((), (), s32[]{:S(2)}) async-start(), calls=%async_computation.3 | async-start | bytes 262144 | tf_op jit(solution)/shard_map/psum | solution.py:124
  15.0 2.4 copy-start.1
  15.0 2.4 copy-start.10
  15.0 2.4 copy-start.13
  17.7 2.1 copy-start.14
  26.3 2.2 copy-start.3
  26.3 2.2 copy-start.7
  28.5 2.4 copy-start.4
  30.6 0.7 copy-start.8
  38.4 2.2 copy-start.3
  38.4 2.2 copy-start.7
  40.7 2.4 copy-start.4
  50.5 2.2 copy-start.3
  50.5 2.2 copy-start.7
  52.8 2.4 copy-start.4
  59.0 36.7 %copy-start.2 = (bf16[32,2048]{1,0:T(8,128)(2,1)S(1)}, bf16[32,2048]{1,0:T(8,128)(2,1)}, u32[]{:S(2)}) copy-start(bf16[32,2048]{1,0:T(8,128)(2,1)} %param.23) | copy-start | bytes 393220
  59.1 37.8 %copy-start.15 = (f32[2048]{0:T(1024)S(1)}, f32[2048]{0:T(1024)}, u32[]{:S(2)}) copy-start(f32[2048]{0:T(1024)} %param.34) | copy-start | bytes 24580
  59.1 39.5 %copy-start.17 = (s32[32,2]{0,1:T(2,128)S(1)}, s32[32,2]{0,1:T(2,128)}, u32[]{:S(2)}) copy-start(s32[32,2]{0,1:T(2,128)} %param.35) | copy-start | bytes 772
  59.1 39.9 %copy-start.16 = (bf16[2048]{0:T(1024)(128)(2,1)S(1)}, bf16[2048]{0:T(1024)(128)(2,1)}, u32[]{:S(2)}) copy-start(bf16[2048]{0:T(1024)(128)(2,1)} %param.40) | copy-start | bytes 12292
  59.1 39.9 %copy-start.23 = (u32[32]{0:T(128)S(1)}, u32[32]{0:T(128)}, u32[]{:S(2)}) copy-start(u32[32]{0:T(128)} %constant.84) | copy-start | bytes 388
  62.8 97.8 %copy-start.21 = (bf16[2048,176]{0,1:T(8,128)(2,1)S(1)}, bf16[2048,176]{0,1:T(8,128)(2,1)}, u32[]{:S(2)}) copy-start(bf16[2048,176]{0,1:T(8,128)(2,1)} %param.41) | copy-start | bytes 2162692
  62.9 97.7 %all-gather.2.cloned.1.call-start = ((), (), s32[]{:S(2)}) async-start(), calls=%async_computation.4 | async-start | bytes 2228224 | tf_op jit(solution)/shard_map/all_gather | solution.py:170
  98.5 155.9 %reduce-scatter.2.cloned.1.call-start = ((), (), s32[]{:S(2)}) async-start(), calls=%async_computation.5 | async-start | bytes 2228224 | tf_op jit(solution)/shard_map/reduce_scatter | solution.py:178
  160.6 2.6 copy-start.19
  160.6 2.6 copy-start.22
  163.2 2.9 %copy-start.9 = (bf16[352,1024]{1,0:T(8,128)(2,1)S(1)}, bf16[352,1024]{1,0:T(8,128)(2,1)}, u32[]{:S(2)}) copy-start(bf16[352,1024]{1,0:T(8,128)(2,1)} %param.43) | copy-start | bytes 2162692
  168.3 39.3 %copy-start.6 = (bf16[1,2048,352]{1,2,0:T(8,128)(2,1)S(1)}, bf16[1,2048,352]{1,2,0:T(8,128)(2,1)}, u32[]{:S(2)}) copy-start(bf16[1,2048,352]{1,2,0:T(8,128)(2,1)} %param.37) | copy-start | bytes 4325380
  168.7 39.5 %copy-start.20 = (bf16[1,2048,352]{1,2,0:T(8,128)(2,1)S(1)}, bf16[1,2048,352]{1,2,0:T(8,128)(2,1)}, u32[]{:S(2)}) copy-start(bf16[1,2048,352]{1,2,0:T(8,128)(2,1)} %param.38) | copy-start | bytes 4325380
  210.8 6.1 %copy-start.12 = (bf16[32,1,2,32]{3,2,0,1:T(2,128)(2,1)S(1)}, bf16[32,1,2,32]{3,2,0,1:T(2,128)(2,1)}, u32[]{:S(2)}) copy-start(bf16[32,1,2,32]{3,2,0,1:T(2,128)(2,1)} %copy-done.11) | copy-start | bytes 12292
  210.8 6.9 %copy-start.18 = (f32[32,2]{0,1:T(2,128)S(1)}, f32[32,2]{0,1:T(2,128)}, u32[]{:S(2)}) copy-start(f32[32,2]{0,1:T(2,128)} %param.36) | copy-start | bytes 772
  212.4 23.7 %all-to-all-start.1 = ((bf16[16,16,1024]{2,1,0:T(8,128)(2,1)}), bf16[16,16,1024]{2,1,0:T(8,128)(2,1)S(1)}, u32[]{:S(2)}, u32[]{:S(2)}) async-start(bf16[16,16,1024]{2,1,0:T(8,128)(2,1)} %fusion.26), calls=%async_computation.1 | async-start | bytes 1048576 | tf_op jit(solution)/shard_map/all_to_all | solution.py:157
  (6 other events, 3.9 us)
Sparse Core Ops, SparseCore 0:
  63.0 32.7 all-reduce.2
  98.6 61.9 all-gather.1
  168.4 85.9 reduce-scatter.1
where the time goes:
time: 263 us
  blocking collectives  85.2 us (32%)
  waiting for transfers between devices  84.9 us (32%)
  matrix products  30.5 us (12%)
  local copies, waits for them, and re-layouts  29 us (11%)
  between operations  15.5 us (6%)
  other arithmetic  13 us (5%)
  starting transfers between devices  4.45 us (2%)
    unnamed x1, blocking collectives  42.2 us
    all_to_all x1, blocking collectives, per_device(): lax.all_to_all(outgoing, 'ep', split_axis=0, concat_axis=0, tiled=True)  38.9 us
    psum x1, waiting for transfers between devices, per_device(): lax.psum(jnp.dot(head_out, w_out, preferred_element_type=jnp.float32).ast...  32.9 us
    dynamic_slice x6, local copies, waits for them, and re-layouts, visit(): lax.dynamic_slice_in_dim(key_cache, offset, span_len, 1)  19.3 us
    all_to_all x1, waiting for transfers between devices, per_device(): lax.all_to_all(partial_value.astype(jnp.bfloat16), 'ep', split_axis=0, co...  18.3 us
    reduce_scatter x1, waiting for transfers between devices, per_device(): lax.psum_scatter(jnp.dot(dense_act, dense_down, preferred_element_type=jn...  18.2 us
    all_gather x1, waiting for transfers between devices, per_device(): lax.all_gather(moe_in, 'ep', axis=0, tiled=True)  15.5 us
    dot_general x3, matrix products, visit(): jnp.einsum('sgaml,slge->sgame', weights.astype(jnp.bfloat16), cached, pre...  6.24 us
  transfers between devices with their start and end apart: 4, of which 4 were waited for; matrix products, arithmetic and copies ran while one was open for 3% of the time, Pallas kernels for 0%

commit v1 on v0

v1 whole, which is shorter than its diff:
```python
import functools

import jax
import jax.numpy as jnp
from jax import lax
from jax.experimental import pallas as pl
from jax.experimental.pallas import tpu as pltpu
from jax.sharding import PartitionSpec as P

HEAD_DIM = 64
VALUE_DIM = 128
EPS = 1e-05
ROPE_BASE = 10000.0
SPAN = 256
GROUP = 4
F32 = jnp.float32
BF16 = jnp.bfloat16
MESH = pl.DeviceIdType.MESH
VMEM = pl.BlockSpec(memory_space=pltpu.VMEM)
ANY = pl.BlockSpec(memory_space=pl.ANY)
SMEM = pl.BlockSpec(memory_space=pltpu.SMEM)


def loop(low, high, body):
    def step(index, carry):
        body(index)
        return carry

    lax.fori_loop(low, high, step, 0)


def attention_kernel(
    lens, hid, cos, sin, again, lam, hgain, wq_any, wk_any, wv_any, wo_any, kc, vc,
    part, kn_out, vn_out,
    wq, wk, wv, wo, kbuf, vbuf, q3, ho3, kn, vn, wsem, csem,
):
    rows = hid.shape[0]
    heads = lam.shape[0]
    spans = kc.shape[1] // SPAN
    groups = rows // GROUP
    loads = [
        pltpu.make_async_copy(src, dst, wsem.at[i])
        for i, (src, dst) in enumerate(((wq_any, wq), (wk_any, wk), (wv_any, wv), (wo_any, wo)))
    ]
    for load in loads[:3]:
        load.start()

    def cache_copies(group, act):
        slot = group % 2
        for i in range(GROUP):
            seq = group * GROUP + i
            need = (lens[seq] + SPAN - 1) // SPAN
            for b in range(spans):
                def both(i=i, seq=seq, b=b):
                    piece = pl.ds(b * SPAN, SPAN)
                    for k, (cache, buf) in enumerate(((kc, kbuf), (vc, vbuf))):
                        act(pltpu.make_async_copy(
                            cache.at[seq, piece, :], buf.at[slot, i, piece, :],
                            csem.at[slot, i, b, k],
                        ))

                pl.when(b < need)(both)

    vbuf[...] = jnp.zeros_like(vbuf)
    cache_copies(0, lambda c: c.start())
    loads[3].start()

    x = hid[...].astype(F32)
    normed = (x * lax.rsqrt(jnp.mean(x * x, axis=-1, keepdims=True) + EPS) * again[...]).astype(BF16)
    lane = lax.broadcasted_iota(jnp.int32, (rows, 128), 1)
    front = (lane % HEAD_DIM) < HEAD_DIM // 2

    def rope(t):
        swapped = jnp.where(front, pltpu.roll(t, 96, 1), pltpu.roll(t, 32, 1))
        return (t * cos[...] + swapped * sin[...]).astype(BF16)

    loads[0].wait()
    for pair in range(heads // 2):
        q = jnp.dot(normed, wq[:, pair * 256:(pair + 1) * 256], preferred_element_type=F32)
        for k in range(2):
            q3[:, pair * 2 + k, :] = rope(q[:, k * 128:(k + 1) * 128]).astype(F32) * (HEAD_DIM ** -0.5)
    loads[1].wait()
    loads[2].wait()
    key = rope(jnp.dot(normed, wk[...], preferred_element_type=F32))
    kn_out[...] = key
    kn[...] = key.astype(F32)
    val = jnp.dot(normed, wv[...], preferred_element_type=F32).astype(BF16)
    vn_out[...] = val
    vn[...] = val.astype(F32)
    lane8 = lax.broadcasted_iota(jnp.int32, (heads, 128), 1)

    def compute(group, width):
        slot = group % 2
        seqs = [group * GROUP + i for i in range(GROUP)]
        owns, scores = [], []
        for i, seq in enumerate(seqs):
            q8 = q3[seq]
            zero = jnp.zeros_like(q8)
            q16 = jnp.concatenate(
                [jnp.where(lane8 < HEAD_DIM, q8, zero), jnp.where(lane8 < HEAD_DIM, zero, q8)], axis=0
            )
            owns.append(jnp.sum(q16 * kn[pl.ds(seq, 1), :], axis=1, keepdims=True))
            scores.append(lax.dot_general(
                q16.astype(BF16), kbuf[slot, i, :width, :], (((1,), (1,)), ((), ())),
                preferred_element_type=F32,
            ))
        place = lax.broadcasted_iota(jnp.int32, scores[0].shape, 1)
        weights, totals, own_weights = [], [], []
        for i, seq in enumerate(seqs):
            s = jnp.where(place < lens[seq], scores[i], -jnp.inf)
            top = jnp.maximum(jnp.max(s, axis=1, keepdims=True), owns[i])
            w = jnp.exp(s - top)
            own = jnp.exp(owns[i] - top)
            totals.append(jnp.sum(w, axis=1, keepdims=True) + own)
            weights.append(w.astype(BF16))
            own_weights.append(own.astype(BF16).astype(F32))
        for i, seq in enumerate(seqs):
            summed = jnp.dot(weights[i], vbuf[slot, i, :width, :], preferred_element_type=F32)
            mapped = (summed + own_weights[i] * vn[pl.ds(seq, 1), :]) / totals[i]
            mix = mapped[:heads] - lam[...] * mapped[heads:]
            ho3[seq] = mix * lax.rsqrt(jnp.mean(mix * mix, axis=-1, keepdims=True) + EPS) * hgain[...]

    def visit(group):
        @pl.when(group + 1 < groups)
        def _():
            cache_copies(group + 1, lambda c: c.start())

        cache_copies(group, lambda c: c.wait())
        longest = lens[group * GROUP]
        for i in range(1, GROUP):
            longest = jnp.maximum(longest, lens[group * GROUP + i])
        need = (longest + SPAN - 1) // SPAN
        for b in range(1, spans + 1):
            pl.when(need == b)(functools.partial(compute, group, b * SPAN))

    loop(0, groups, visit)
    ho = jnp.concatenate([ho3[:, a, :] for a in range(heads)], axis=1).astype(BF16)
    loads[3].wait()
    width = wo.shape[1]
    for t in range(width // 512):
        cols = slice(t * 512, (t + 1) * 512)
        part[:, cols] = jnp.dot(ho, wo[:, cols], preferred_element_type=F32).astype(BF16)


def ffn_kernel(
    n, zs,
    part, hid, fgain, wt, gvec, eg_any, eu_any, ed_any, dg_any, du_any, dd_any,
    out,
    eg, eu, ed, dg, du, dd, peer, res, rows, wtb, eact, dact, sp, rp, zsend, zrecv, own,
    wsem, psem, rsend, rrecv, zs_send, pl_send, arr, fw_send, fw_recv, as_send, as_recv,
    sp_send, rp_recv, zq_send, zq_recv,
):
    ms = n // zs
    batch = hid.shape[0]
    half = hid.shape[1] // 2
    me = lax.axis_index("ep")
    c = lax.axis_index("tp")
    z, p = me // ms, me % ms
    other = (me, 1 - c)

    loads = [
        pltpu.make_async_copy(src, dst, wsem.at[i])
        for i, (src, dst) in enumerate((
            (eg_any.at[0], eg), (eu_any.at[0], eu), (dg_any, dg), (du_any, du),
            (ed_any.at[0], ed), (dd_any, dd),
        ))
    ]
    for load in loads:
        load.start()

    barrier = pltpu.get_barrier_semaphore()

    def greet(k):
        pl.semaphore_signal(barrier, inc=1, device_id=((me + k) % n, c), device_id_type=MESH)

    pl.semaphore_signal(barrier, inc=1, device_id=other, device_id_type=MESH)
    loop(1, n, greet)
    pl.semaphore_wait(barrier, n)

    def remote(src, dst, send, recv, where):
        return pltpu.make_async_remote_copy(
            src_ref=src, dst_ref=dst, send_sem=send, recv_sem=recv,
            device_id=where, device_id_type=MESH,
        )

    swap = remote(part, peer, psem.at[0], psem.at[1], other)
    swap.start()

    def route(k):
        return remote(wt, wtb.at[me], rsend.at[k], rrecv.at[me], ((me + k) % n, c))

    loop(1, n, lambda k: route(k).start())
    wtb[me] = wt[...]
    swap.wait()
    attn = (part[...].astype(F32) + peer[...].astype(F32)).astype(BF16).astype(F32)
    residual = hid[...].astype(F32) + attn
    res[...] = residual
    moe = (
        residual * lax.rsqrt(jnp.mean(residual * residual, axis=-1, keepdims=True) + EPS) * fgain[...]
    ).astype(BF16)
    rows[0, me] = moe[:, :half]
    rows[1, me] = moe[:, half:]

    def zcopy(d):
        return remote(rows.at[c, me], rows.at[c, me], zs_send.at[d], arr.at[me], (((z + d) % zs) * ms + p, c))

    def plane(d, k):
        slot = ((z + d) % zs) * ms + p
        return remote(
            rows.at[c, slot], rows.at[c, slot], pl_send.at[d, k], arr.at[slot], (z * ms + (p + k) % ms, c)
        )

    def forward(slot):
        return remote(rows.at[c, slot], rows.at[c, slot], fw_send.at[slot], fw_recv.at[slot], other)

    def arrival(slot):
        return remote(rows.at[c, slot], rows.at[c, slot], fw_send.at[slot], arr.at[slot], other)

    def partner_arrival(slot):
        return remote(rows.at[1 - c, slot], rows.at[1 - c, slot], fw_send.at[slot], fw_recv.at[slot], other)

    loop(1, zs, lambda d: zcopy(d).start())
    loop(1, ms, lambda k: plane(0, k).start())

    def relay(d):
        slot = ((z + d) % zs) * ms + p
        arrival(slot).wait_recv()
        loop(1, ms, lambda k: plane(d, k).start())
        forward(slot).start()

    loop(1, zs, relay)
    for load in loads:
        load.wait()

    def acts(d, buf, k):
        zd = (z + d) % zs
        return remote(buf.at[c, zd], buf.at[c, zd], as_send.at[k, zd], as_recv.at[k, zd], other)

    def first(d):
        zd = (z + d) % zs

        def take(k):
            slot = zd * ms + (p + k) % ms
            arrival(slot).wait_recv()
            forward(slot).start()

        loop(1, ms, take)

        def met(k):
            slot = zd * ms + (p + k) % ms

            @pl.when(slot != me)
            def _():
                partner_arrival(slot).wait_recv()

        loop(0, ms, met)
        block = pl.ds(zd * ms, ms)
        left = rows[0, block].reshape(ms * batch, half)
        right = rows[1, block].reshape(ms * batch, half)

        def both(w):
            return jnp.dot(left, w[:half, :], preferred_element_type=F32) + jnp.dot(
                right, w[half:, :], preferred_element_type=F32
            )

        for buf, gate, up in ((eact, eg, eu), (dact, dg, du)):
            g = both(gate)
            buf[c, zd] = (g / (1.0 + jnp.exp(-g)) * both(up)).astype(BF16)
        acts(d, eact, 0).start()
        acts(d, dact, 1).start()

    loop(0, zs, first)
    loop(1, n, lambda k: remote(
        wt, wtb.at[(me + k) % n], rsend.at[k], rrecv.at[(me + k) % n], other).wait_recv())
    expert = me // 2
    lane = lax.broadcasted_iota(jnp.int32, (batch, 128), 1)
    line = lax.broadcasted_iota(jnp.int32, (batch, 128), 0)

    def send_part(zd, k):
        q = (p + k) % ms
        return remote(sp.at[zd, q], rp.at[zd, p], sp_send.at[zd, k], rp_recv.at[zd, p], (z * ms + q, c))

    def part_arrival(zd, k):
        q = (p + k) % ms
        return remote(sp.at[zd, q], rp.at[zd, q], sp_send.at[zd, k], rp_recv.at[zd, q], (z * ms + q, c))

    def second(i):
        d = (i + 1) % zs
        zd = (z + d) % zs
        for k, buf in enumerate((eact, dact)):
            remote(buf.at[1 - c, zd], buf.at[1 - c, zd], as_send.at[k, zd], as_recv.at[k, zd], other).wait_recv()
        block = pl.ds(zd * ms, ms)
        gate = (
            jnp.sum(rows[0, block].reshape(ms * batch, half).astype(F32) * gvec[:, :half], axis=1, keepdims=True)
            + jnp.sum(rows[1, block].reshape(ms * batch, half).astype(F32) * gvec[:, half:], axis=1, keepdims=True)
        )
        gate = (1.0 / (1.0 + jnp.exp(-gate))).astype(BF16).astype(F32)
        share = jnp.concatenate([
            jnp.sum(jnp.where(lane == line, wtb[zd * ms + q, pl.ds(expert, 1), :], 0.0), axis=1, keepdims=True)
            for q in range(ms)
        ], axis=0)
        ew, dw = eact.shape[-1], dact.shape[-1]
        y = share * (
            jnp.dot(eact[0, zd], ed[:ew, :], preferred_element_type=F32)
            + jnp.dot(eact[1, zd], ed[ew:, :], preferred_element_type=F32)
        ) + gate * (
            jnp.dot(dact[0, zd], dd[:dw, :], preferred_element_type=F32)
            + jnp.dot(dact[1, zd], dd[dw:, :], preferred_element_type=F32)
        )
        sp[zd] = y.astype(BF16).reshape(ms, batch, half)
        loop(1, ms, lambda k: send_part(zd, k).start())

    loop(0, zs, second)

    def gathered(zd):
        loop(1, ms, lambda k: part_arrival(zd, k).wait_recv())
        total = sp[zd, p].astype(F32)
        for k in range(1, ms):
            total = total + rp[zd, (p + k) % ms].astype(F32)
        return total

    def zback(d):
        zd = (z + d) % zs
        return remote(zsend.at[zd], zrecv.at[z], zq_send.at[d], zq_recv.at[z], (zd * ms + p, c))

    def third(d):
        zd = (z + d) % zs
        zsend[zd] = gathered(zd).astype(BF16)
        zback(d).start()

    loop(1, zs, third)
    own[...] = gathered(z) + res[:, pl.ds(pl.multiple_of(c * half, half), half)]

    def last(d):
        zd = (z + d) % zs
        remote(zsend.at[zd], zrecv.at[zd], zq_send.at[d], zq_recv.at[zd], other).wait_recv()
        own[...] += zrecv[zd].astype(F32)

    loop(1, zs, last)
    out[...] = own[...].astype(BF16)

    loop(1, n, lambda k: route(k).wait_send())
    loop(1, zs, lambda d: zcopy(d).wait_send())

    def settle(d):
        loop(1, ms, lambda k: plane(d, k).wait_send())
        acts(d, eact, 0).wait_send()
        acts(d, dact, 1).wait_send()
        zd = (z + d) % zs
        loop(1, ms, lambda k: send_part(zd, k).wait_send())

    loop(0, zs, settle)
    loop(1, n, lambda k: forward((me + k) % n).wait_send())
    loop(1, zs, lambda d: zback(d).wait_send())


def per_device(
    n_ep, hidden_in, past_lengths, key_cache, value_cache, attn_gain, w_query, w_key, w_value, lambdas,
    head_gain, w_out, ffn_gain, route_ids, route_weights, expert_gate, expert_up, expert_down,
    gate_vector, dense_gate, dense_up, dense_down,
):
    batch, width = hidden_in.shape
    half = width // 2
    heads = lambdas.shape[0]
    cache_len = key_cache.shape[1]
    middle = HEAD_DIM // 2
    inverse = ROPE_BASE ** (-jnp.arange(middle, dtype=F32) / middle)
    angles = past_lengths.astype(F32)[:, None] * inverse[None, :]
    cosine, sine = jnp.cos(angles), jnp.sin(angles)
    cos = jnp.concatenate([cosine] * 4, axis=1)
    sin = jnp.concatenate([-sine, sine] * 2, axis=1)
    sem = pltpu.SemaphoreType.DMA
    part, key_new, value_new = pl.pallas_call(
        attention_kernel,
        out_shape=(
            jax.ShapeDtypeStruct((batch, width), BF16),
            jax.ShapeDtypeStruct((batch, 128), BF16),
            jax.ShapeDtypeStruct((batch, 128), BF16),
        ),
        in_specs=[SMEM] + [VMEM] * 6 + [ANY] * 6,
        out_specs=(VMEM, VMEM, VMEM),
        scratch_shapes=[
            pltpu.VMEM(w_query.shape, BF16),
            pltpu.VMEM(w_key.shape, BF16),
            pltpu.VMEM(w_value.shape, BF16),
            pltpu.VMEM(w_out.shape, BF16),
            pltpu.VMEM((2, GROUP, cache_len, 128), BF16),
            pltpu.VMEM((2, GROUP, cache_len, 128), BF16),
            pltpu.VMEM((batch, heads, 128), F32),
            pltpu.VMEM((batch, heads, 128), F32),
            pltpu.VMEM((batch, 128), F32),
            pltpu.VMEM((batch, 128), F32),
            sem((4,)),
            sem((2, GROUP, cache_len // SPAN, 2)),
        ],
        name="attend",
    )(
        past_lengths, hidden_in, cos, sin, attn_gain.reshape(1, -1), lambdas.reshape(-1, 1),
        head_gain.reshape(1, -1), w_query, w_key, w_value, w_out, key_cache, value_cache,
    )
    experts = n_ep // 2
    named = route_ids.T[None, :, :] == jnp.arange(experts)[:, None, None]
    table = jnp.sum(jnp.where(named, route_weights.T[None, :, :], 0.0), axis=1)
    table = jnp.pad(table, ((0, 0), (0, 128 - batch)))
    zs = 4 if n_ep % 4 == 0 else 1
    ms = n_ep // zs
    expert_w, dense_w = expert_gate.shape[2], dense_gate.shape[1]
    mixed = pl.pallas_call(
        functools.partial(ffn_kernel, n_ep, zs),
        out_shape=jax.ShapeDtypeStruct((batch, half), BF16),
        in_specs=[VMEM] * 5 + [ANY] * 6,
        out_specs=VMEM,
        scratch_shapes=[
            pltpu.VMEM(expert_gate.shape[1:], BF16),
            pltpu.VMEM(expert_up.shape[1:], BF16),
            pltpu.VMEM(expert_down.shape[1:], BF16),
            pltpu.VMEM(dense_gate.shape, BF16),
            pltpu.VMEM(dense_up.shape, BF16),
            pltpu.VMEM(dense_down.shape, BF16),
            pltpu.VMEM((batch, width), BF16),
            pltpu.VMEM((batch, width), F32),
            pltpu.VMEM((2, n_ep, batch, half), BF16),
            pltpu.VMEM((n_ep, experts, 128), F32),
            pltpu.VMEM((2, zs, ms * batch, expert_w), BF16),
            pltpu.VMEM((2, zs, ms * batch, dense_w), BF16),
            pltpu.VMEM((zs, ms, batch, half), BF16),
            pltpu.VMEM((zs, ms, batch, half), BF16),
            pltpu.VMEM((zs, batch, half), BF16),
            pltpu.VMEM((zs, batch, half), BF16),
            pltpu.VMEM((batch, half), F32),
            sem((6,)), sem((2,)), sem((n_ep,)), sem((n_ep,)), sem((zs,)), sem((zs, ms)), sem((n_ep,)),
            sem((n_ep,)), sem((n_ep,)), sem((2, zs)), sem((2, zs)), sem((zs, ms)), sem((zs, ms)),
            sem((zs,)), sem((zs,)),
        ],
        compiler_params=pltpu.CompilerParams(collective_id=0, has_side_effects=True),
        name="feed",
    )(
        part, hidden_in, ffn_gain.reshape(1, -1), table, gate_vector.astype(F32).reshape(1, -1),
        expert_gate, expert_up, expert_down, dense_gate, dense_up, dense_down,
    )
    return mixed, key_new, value_new


def solution(mesh):
    return jax.shard_map(
        functools.partial(per_device, mesh.shape["ep"]),
        mesh=mesh,
        in_specs=(
            P("ep", None),
            P("ep"),
            P("ep", None, "tp"),
            P("ep", None, "tp"),
            P(),
            P(None, "tp"),
            P(None, "tp"),
            P(None, "tp"),
            P("tp"),
            P(),
            P("tp", None),
            P(),
            P("ep", None),
            P("ep", None),
            P("ep", None, "tp"),
            P("ep", None, "tp"),
            P("ep", None, "tp"),
            P(),
            P(None, ("ep", "tp")),
            P(None, ("ep", "tp")),
            P("ep", "tp"),
        ),
        out_specs=(P("ep", "tp"), P("ep", "tp"), P("ep", "tp")),
        check_vma=False,
    )
```

time: 263 us -> 75.3 us (0.29)
  blocking collectives: 85.2 us -> 0 us
  waiting for transfers between devices: 84.9 us -> 0 us
  Pallas kernels: 0 us -> 61.7 us
  matrix products: 30.5 us -> 0 us
  local copies, waits for them, and re-layouts: 29 us -> 9.13 us
  between operations: 15.5 us -> 0.68 us
  other arithmetic: 13 us -> 3.5 us
  starting transfers between devices: 4.45 us -> 0 us
    pallas_call x0 -> x2, Pallas kernels: none -> 61.7 us  [the longest x1 47.3 us: per_device(): pl.pallas_call(functools.partial(ffn_kernel, n_ep, zs), out_shape=jax.Sha...]
    unnamed x1 -> x0, blocking collectives: 42.2 us -> none
    all_to_all x1 -> x0, blocking collectives: 38.9 us -> none  [per_device(): lax.all_to_all(outgoing, 'ep', split_axis=0, concat_axis=0, tiled=True)]
    psum x1 -> x0, waiting for transfers between devices: 32.9 us -> none  [per_device(): lax.psum(jnp.dot(head_out, w_out, preferred_element_type=jnp.float32).ast...]
    dot_general x20 -> x0, matrix products: 30.5 us -> none  [the longest x3 6.24 us: visit(): jnp.einsum('sgaml,slge->sgame', weights.astype(jnp.bfloat16), cached, pre...]
    dynamic_slice x6 -> x0, local copies, waits for them, and re-layouts: 19.3 us -> none  [visit(): lax.dynamic_slice_in_dim(key_cache, offset, span_len, 1)]
    all_to_all x1 -> x0, waiting for transfers between devices: 18.3 us -> none  [per_device(): lax.all_to_all(partial_value.astype(jnp.bfloat16), 'ep', split_axis=0, co...]
    reduce_scatter x1 -> x0, waiting for transfers between devices: 18.2 us -> none  [per_device(): lax.psum_scatter(jnp.dot(dense_act, dense_down, preferred_element_type=jn...]
  transfers between devices with their start and end apart: 4 -> 0, of which waited for: 4 -> 0; matrix products, arithmetic and copies ran while one was open for 3% -> 0% of each run, Pallas kernels for 0% -> 0%
where the time goes in v1:
time: 75.3 us; the launch traced here: 75 us
  Pallas kernels  61.7 us (82%)
  local copies, waits for them, and re-layouts  9.13 us (12%)
  other arithmetic  3.5 us (5%)
    pallas_call x1, Pallas kernels, per_device(): pl.pallas_call(functools.partial(ffn_kernel, n_ep, zs), out_shape=jax.Sha...  47.3 us
    pallas_call x1, Pallas kernels, per_device(): pl.pallas_call(attention_kernel, out_shape=(jax.ShapeDtypeStruct((batch,...  14.4 us
    unnamed x13, local copies, waits for them, and re-layouts  7.21 us

profile of v1, /device:TPU:0, one launch (start us, length us, event | category | flops | bytes accessed | tf_op | source)
XLA Modules:
  0.0 75.0 jit_solution(10883264602637067624)
XLA Ops:
  0.6 0.7 convert_element_type.6
  1.3 1.3 %copy.29.lam = f32[8,1]{1,0:T(8,128)} copy(f32[8,1]{0,1:T(1,128)} %bitcast.13) | data formatting | bytes 64 | tf_op jit(solution)/shard_map/reshape | solution.py:398
  2.6 0.7 select_reduce_fusion
  3.3 0.6 pad.4.wt
  3.9 1.3 %reshape.38 = f32[2048]{0:T(1024)} convert(bf16[2048]{0:T(1024)(128)(2,1)} %param.38) | non-fusion elementwise | flops 2048 | bytes 12288 | tf_op jit(solution)/shard_map/reshape | solution.py:438
  5.2 0.1 fusion
  5.3 0.7 pad_maximum_fusion
  6.1 0.0 copy-start.2
  6.1 14.4 %attend.1 = (bf16[32,2048]{1,0:T(8,128)(2,1)}, bf16[32,128]{1,0:T(8,128)(2,1)}, bf16[32,128]{1,0:T(8,128)(2,1)}) custom-call(s32[32]{0:T(128)} %lens.1, bf16[32,2048]{1,0:T(8,128)(2,1)} %hid.3, f32[32,128]{1,0:T(8,128)} %get-tuple-element.12.cos, f32[32,128]{1,0:T(8,128)} %get-tuple-element.13.sin, f32[1,2048]{1,0:T(1,128)} %bitcast.8, f32[8,1]{1,0:T(8,128)} %copy.29.lam, ...), custom_call_target="tpu_custom_call" | custom-call | tf_op jit(solution)/shard_map/attend/pallas_call | solution.py:373
  20.4 0.0 copy-start.3
  20.4 0.0 copy-done.2
  20.5 0.0 copy-start
  20.5 1.3 %copy.32.dg_any = bf16[2048,176]{1,0:T(8,128)(2,1)} copy(bf16[2048,176]{0,1:T(8,128)(2,1)S(1)} %copy-done.2) | data formatting | bytes 1441792 | tf_op args[18]
  21.8 0.0 copy-done.3
  21.8 1.3 %copy.33.du_any = bf16[2048,176]{1,0:T(8,128)(2,1)} copy(bf16[2048,176]{0,1:T(8,128)(2,1)S(1)} %copy-done.3) | data formatting | bytes 1441792 | tf_op args[19]
  23.1 0.0 copy-done
  23.1 0.0 copy-start.1
  23.1 1.6 %copy.30.eg_any = bf16[1,2048,352]{2,1,0:T(8,128)(2,1)} copy(bf16[1,2048,352]{1,2,0:T(8,128)(2,1)S(1)} %copy-done) | data formatting | bytes 2883584 | tf_op args[14]
  24.6 0.0 copy-done.1
  24.6 1.6 %copy.31.eu_any = bf16[1,2048,352]{2,1,0:T(8,128)(2,1)} copy(bf16[1,2048,352]{1,2,0:T(8,128)(2,1)S(1)} %copy-done.1) | data formatting | bytes 2883584 | tf_op args[15]
  26.2 47.3 %feed.1 = bf16[32,1024]{1,0:T(8,128)(2,1)} custom-call(bf16[32,2048]{1,0:T(8,128)(2,1)} %get-tuple-element.6.part, bf16[32,2048]{1,0:T(8,128)(2,1)} %hid.3, f32[1,2048]{1,0:T(1,128)} %bitcast.9, f32[8,128]{1,0:T(8,128)} %pad.4.wt, f32[1,2048]{1,0:T(1,128)} %bitcast.7, bf16[1,2048,352]{2,1,0:T(8,128)(2,1)} %copy.30.eg_any, ...), custom_call_target="tpu_custom_call" | custom-call | tf_op jit(solution)/shard_map/feed/pallas_call | solution.py:408
  73.5 1.5 %copy.35 = bf16[32,1024]{1,0:T(8,128)(2,1)} copy(bf16[32,1024]{1,0:T(8,128)(2,1)} %feed.1) | data formatting | bytes 131072
  (1 shorter events, 0.0 us)
Async XLA Ops:
  6.1 14.4 %copy-start.2 = (bf16[2048,176]{0,1:T(8,128)(2,1)S(1)}, bf16[2048,176]{0,1:T(8,128)(2,1)}, u32[]{:S(2)}) copy-start(bf16[2048,176]{0,1:T(8,128)(2,1)} %param.39) | copy-start | bytes 2162692
  20.4 1.3 %copy-start.3 = (bf16[2048,176]{0,1:T(8,128)(2,1)S(1)}, bf16[2048,176]{0,1:T(8,128)(2,1)}, u32[]{:S(2)}) copy-start(bf16[2048,176]{0,1:T(8,128)(2,1)} %param.40) | copy-start | bytes 2162692
  20.5 2.6 %copy-start = (bf16[1,2048,352]{1,2,0:T(8,128)(2,1)S(1)}, bf16[1,2048,352]{1,2,0:T(8,128)(2,1)}, u32[]{:S(2)}) copy-start(bf16[1,2048,352]{1,2,0:T(8,128)(2,1)} %param.35) | copy-start | bytes 4325380
  23.1 1.6 %copy-start.1 = (bf16[1,2048,352]{1,2,0:T(8,128)(2,1)S(1)}, bf16[1,2048,352]{1,2,0:T(8,128)(2,1)}, u32[]{:S(2)}) copy-start(bf16[1,2048,352]{1,2,0:T(8,128)(2,1)} %param.36) | copy-start | bytes 4325380

commit v2 on v1

--- a/solution.py
+++ b/solution.py
@@ -2,6 +2,7 @@
 
 import jax
 import jax.numpy as jnp
+import numpy as np
 from jax import lax
 from jax.experimental import pallas as pl
 from jax.experimental.pallas import tpu as pltpu
@@ -29,8 +30,15 @@
     lax.fori_loop(low, high, step, 0)
 
 
+def column(row, count):
+    spread = (count, row.shape[1])
+    lane = lax.broadcasted_iota(jnp.int32, spread, 1)
+    line = lax.broadcasted_iota(jnp.int32, spread, 0)
+    return jnp.sum(jnp.where(lane == line, row.astype(F32), 0.0), axis=1, keepdims=True)
+
+
 def attention_kernel(
-    lens, hid, cos, sin, again, lam, hgain, wq_any, wk_any, wv_any, wo_any, kc, vc,
+    lens, lam, lens_row, inverse, hid, again, hgain, wq_any, wk_any, wv_any, wo_any, kc, vc,
     part, kn_out, vn_out,
     wq, wk, wv, wo, kbuf, vbuf, q3, ho3, kn, vn, wsem, csem,
 ):
@@ -70,9 +78,13 @@
     lane = lax.broadcasted_iota(jnp.int32, (rows, 128), 1)
     front = (lane % HEAD_DIM) < HEAD_DIM // 2
 
+    angles = column(lens_row[...], rows) * inverse[...]
+    cos, sin = jnp.cos(angles), jnp.sin(angles)
+    sin = jnp.where(front, -sin, sin)
+
     def rope(t):
         swapped = jnp.where(front, pltpu.roll(t, 96, 1), pltpu.roll(t, 32, 1))
-        return (t * cos[...] + swapped * sin[...]).astype(BF16)
+        return (t * cos + swapped * sin).astype(BF16)
 
     loads[0].wait()
     for pair in range(heads // 2):
@@ -88,6 +100,10 @@
     vn_out[...] = val
     vn[...] = val.astype(F32)
     lane8 = lax.broadcasted_iota(jnp.int32, (heads, 128), 1)
+    line8 = lax.broadcasted_iota(jnp.int32, (heads, 128), 0)
+    lam8 = jnp.zeros((heads, 128), F32)
+    for a in range(heads):
+        lam8 = jnp.where(line8 == a, lam[a], lam8)
 
     def compute(group, width):
         slot = group % 2
@@ -117,7 +133,7 @@
         for i, seq in enumerate(seqs):
             summed = jnp.dot(weights[i], vbuf[slot, i, :width, :], preferred_element_type=F32)
             mapped = (summed + own_weights[i] * vn[pl.ds(seq, 1), :]) / totals[i]
-            mix = mapped[:heads] - lam[...] * mapped[heads:]
+            mix = mapped[:heads] - lam8 * mapped[heads:]
             ho3[seq] = mix * lax.rsqrt(jnp.mean(mix * mix, axis=-1, keepdims=True) + EPS) * hgain[...]
 
     def visit(group):
@@ -144,10 +160,10 @@
 
 def ffn_kernel(
     n, zs,
-    part, hid, fgain, wt, gvec, eg_any, eu_any, ed_any, dg_any, du_any, dd_any,
+    part, hid, fgain, ids, shares, gvec, eg_any, eu_any, ed_any, dg_any, du_any, dd_any,
     out,
     eg, eu, ed, dg, du, dd, peer, res, rows, wtb, eact, dact, sp, rp, zsend, zrecv, own,
-    wsem, psem, rsend, rrecv, zs_send, pl_send, arr, fw_send, fw_recv, as_send, as_recv,
+    wsem, psem, rsend, rrecv, zs_send, pl_send, hop_send, arr, fw_send, fw_recv, as_send, as_recv,
     sp_send, rp_recv, zq_send, zq_recv,
 ):
     ms = n // zs
@@ -168,7 +184,18 @@
     for load in loads:
         load.start()
 
+    experts = wtb.shape[1]
+    numbers = lax.broadcasted_iota(jnp.int32, (experts, batch), 0)
+    table = jnp.zeros((experts, batch), F32)
+    for k in range(ids.shape[0]):
+        table = table + jnp.where(ids[k:k + 1, :] == numbers, shares[k:k + 1, :], 0.0)
+    wtb[me] = jnp.pad(table, ((0, 0), (0, 128 - batch)))
     barrier = pltpu.get_barrier_semaphore()
+
+    quad = ms == 4
+
+    def flip(q, bit):
+        return q + bit - 2 * bit * ((q // bit) % 2)
 
     def greet(k):
         pl.semaphore_signal(barrier, inc=1, device_id=((me + k) % n, c), device_id_type=MESH)
@@ -187,10 +214,9 @@
     swap.start()
 
     def route(k):
-        return remote(wt, wtb.at[me], rsend.at[k], rrecv.at[me], ((me + k) % n, c))
+        return remote(wtb.at[me], wtb.at[me], rsend.at[k], rrecv.at[me], ((me + k) % n, c))
 
     loop(1, n, lambda k: route(k).start())
-    wtb[me] = wt[...]
     swap.wait()
     attn = (part[...].astype(F32) + peer[...].astype(F32)).astype(BF16).astype(F32)
     residual = hid[...].astype(F32) + attn
@@ -210,6 +236,12 @@
             rows.at[c, slot], rows.at[c, slot], pl_send.at[d, k], arr.at[slot], (z * ms + (p + k) % ms, c)
         )
 
+    def plane4(d, bit):
+        slot = ((z + d) % zs) * ms + p
+        return remote(
+            rows.at[c, slot], rows.at[c, slot], pl_send.at[d, bit], arr.at[slot], (z * ms + flip(p, bit), c)
+        )
+
     def forward(slot):
         return remote(rows.at[c, slot], rows.at[c, slot], fw_send.at[slot], fw_recv.at[slot], other)
 
@@ -220,17 +252,47 @@
         return remote(rows.at[1 - c, slot], rows.at[1 - c, slot], fw_send.at[slot], fw_recv.at[slot], other)
 
     loop(1, zs, lambda d: zcopy(d).start())
-    loop(1, ms, lambda k: plane(0, k).start())
-
-    def relay(d):
+
+    near = 1 + c
+    far = 2 - c
+
+    def hop(slot):
+        return remote(
+            rows.at[c, slot], rows.at[c, slot], hop_send.at[slot // ms], arr.at[slot],
+            (z * ms + flip(p, far), c),
+        )
+
+    def spread(d):
         slot = ((z + d) % zs) * ms + p
+
+        @pl.when(d > 0)
+        def _():
+            arrival(slot).wait_recv()
+
+        if quad:
+            plane4(d, 1).start()
+            plane4(d, 2).start()
+        else:
+            loop(1, ms, lambda k: plane(d, k).start())
+
+        @pl.when(d > 0)
+        def _():
+            forward(slot).start()
+
+    def taken(slot):
         arrival(slot).wait_recv()
-        loop(1, ms, lambda k: plane(d, k).start())
         forward(slot).start()
 
-    loop(1, zs, relay)
-    for load in loads:
-        load.wait()
+    def collect(d):
+        base = ((z + d) % zs) * ms
+        if quad:
+            slot = base + flip(p, near)
+            arrival(slot).wait_recv()
+            hop(slot).start()
+            forward(slot).start()
+            taken(base + flip(p, far))
+        else:
+            loop(1, ms, lambda k: taken(base + (p + k) % ms))
 
     def acts(d, buf, k):
         zd = (z + d) % zs
@@ -238,13 +300,8 @@
 
     def first(d):
         zd = (z + d) % zs
-
-        def take(k):
-            slot = zd * ms + (p + k) % ms
-            arrival(slot).wait_recv()
-            forward(slot).start()
-
-        loop(1, ms, take)
+        if quad:
+            taken(zd * ms + 3 - p)
 
         def met(k):
             slot = zd * ms + (p + k) % ms
@@ -259,8 +316,9 @@
         right = rows[1, block].reshape(ms * batch, half)
 
         def both(w):
-            return jnp.dot(left, w[:half, :], preferred_element_type=F32) + jnp.dot(
-                right, w[half:, :], preferred_element_type=F32
+            across = (((1,), (1,)), ((), ()))
+            return lax.dot_general(left, w[:, :half], across, preferred_element_type=F32) + lax.dot_general(
+                right, w[:, half:], across, preferred_element_type=F32
             )
 
         for buf, gate, up in ((eact, eg, eu), (dact, dg, du)):
@@ -269,12 +327,30 @@
         acts(d, eact, 0).start()
         acts(d, dact, 1).start()
 
-    loop(0, zs, first)
+    spread(0)
+
+    def gather_step(d):
+        @pl.when(d + 1 < zs)
+        def _():
+            spread(d + 1)
+
+        @pl.when(d < zs)
+        def _():
+            collect(d)
+
+        @pl.when(d == 1)
+        def _():
+            for load in loads:
+                load.wait()
+
+        @pl.when(d > 0)
+        def _():
+            first(d - 1)
+
+    loop(0, zs + 1, gather_step)
     loop(1, n, lambda k: remote(
-        wt, wtb.at[(me + k) % n], rsend.at[k], rrecv.at[(me + k) % n], other).wait_recv())
+        wtb.at[me], wtb.at[(me + k) % n], rsend.at[k], rrecv.at[(me + k) % n], other).wait_recv())
     expert = me // 2
-    lane = lax.broadcasted_iota(jnp.int32, (batch, 128), 1)
-    line = lax.broadcasted_iota(jnp.int32, (batch, 128), 0)
 
     def send_part(zd, k):
         q = (p + k) % ms
@@ -283,6 +359,24 @@
     def part_arrival(zd, k):
         q = (p + k) % ms
         return remote(sp.at[zd, q], rp.at[zd, q], sp_send.at[zd, k], rp_recv.at[zd, q], (z * ms + q, c))
+
+    def first_leg(zd, k):
+        to = flip(p, near)
+        return remote(
+            sp.at[zd, 3 - p if k == 0 else to], rp.at[zd, k], sp_send.at[zd, k], rp_recv.at[zd, k],
+            (z * ms + to, c),
+        )
+
+    def next_leg(zd):
+        return remote(
+            rp.at[zd, 3], rp.at[zd, 2], sp_send.at[zd, 2], rp_recv.at[zd, 2], (z * ms + flip(p, far), c)
+        )
+
+    def pass_on(i):
+        zd = (z + i + 1) % zs
+        first_leg(zd, 0).wait_recv()
+        rp[zd, 3] = (sp[zd, flip(p, far)].astype(F32) + rp[zd, 0].astype(F32)).astype(BF16)
+        next_leg(zd).start()
 
     def second(i):
         d = (i + 1) % zs
@@ -291,13 +385,12 @@
             remote(buf.at[1 - c, zd], buf.at[1 - c, zd], as_send.at[k, zd], as_recv.at[k, zd], other).wait_recv()
         block = pl.ds(zd * ms, ms)
         gate = (
-            jnp.sum(rows[0, block].reshape(ms * batch, half).astype(F32) * gvec[:, :half], axis=1, keepdims=True)
-            + jnp.sum(rows[1, block].reshape(ms * batch, half).astype(F32) * gvec[:, half:], axis=1, keepdims=True)
+            jnp.sum(rows[0, block].reshape(ms * batch, half).astype(F32) * gvec[:, :half].astype(F32), axis=1, keepdims=True)
+            + jnp.sum(rows[1, block].reshape(ms * batch, half).astype(F32) * gvec[:, half:].astype(F32), axis=1, keepdims=True)
         )
         gate = (1.0 / (1.0 + jnp.exp(-gate))).astype(BF16).astype(F32)
         share = jnp.concatenate([
-            jnp.sum(jnp.where(lane == line, wtb[zd * ms + q, pl.ds(expert, 1), :], 0.0), axis=1, keepdims=True)
-            for q in range(ms)
+            column(wtb[zd * ms + q, pl.ds(expert, 1), :], batch) for q in range(ms)
         ], axis=0)
         ew, dw = eact.shape[-1], dact.shape[-1]
         y = share * (
@@ -308,11 +401,17 @@
             + jnp.dot(dact[1, zd], dd[dw:, :], preferred_element_type=F32)
         )
         sp[zd] = y.astype(BF16).reshape(ms, batch, half)
-        loop(1, ms, lambda k: send_part(zd, k).start())
-
-    loop(0, zs, second)
+        if quad:
+            first_leg(zd, 0).start()
+            first_leg(zd, 1).start()
+        else:
+            loop(1, ms, lambda k: send_part(zd, k).start())
 
     def gathered(zd):
+        if quad:
+            first_leg(zd, 1).wait_recv()
+            next_leg(zd).wait_recv()
+            return sp[zd, p].astype(F32) + rp[zd, 1].astype(F32) + rp[zd, 2].astype(F32)
         loop(1, ms, lambda k: part_arrival(zd, k).wait_recv())
         total = sp[zd, p].astype(F32)
         for k in range(1, ms):
@@ -328,7 +427,21 @@
         zsend[zd] = gathered(zd).astype(BF16)
         zback(d).start()
 
-    loop(1, zs, third)
+    def reduce_step(i):
+        @pl.when(i < zs)
+        def _():
+            second(i)
+
+        if quad:
+            @pl.when((i > 0) & (i <= zs))
+            def _():
+                pass_on(i - 1)
+
+        @pl.when((i > 1) & (i <= zs))
+        def _():
+            third(i - 1)
+
+    loop(0, zs + 1, reduce_step)
     own[...] = gathered(z) + res[:, pl.ds(pl.multiple_of(c * half, half), half)]
 
     def last(d):
@@ -343,11 +456,19 @@
     loop(1, zs, lambda d: zcopy(d).wait_send())
 
     def settle(d):
-        loop(1, ms, lambda k: plane(d, k).wait_send())
+        zd = (z + d) % zs
+        if quad:
+            plane4(d, 1).wait_send()
+            plane4(d, 2).wait_send()
+            hop(zd * ms + flip(p, near)).wait_send()
+            first_leg(zd, 0).wait_send()
+            first_leg(zd, 1).wait_send()
+            next_leg(zd).wait_send()
+        else:
+            loop(1, ms, lambda k: plane(d, k).wait_send())
+            loop(1, ms, lambda k: send_part(zd, k).wait_send())
         acts(d, eact, 0).wait_send()
         acts(d, dact, 1).wait_send()
-        zd = (z + d) % zs
-        loop(1, ms, lambda k: send_part(zd, k).wait_send())
 
     loop(0, zs, settle)
     loop(1, n, lambda k: forward((me + k) % n).wait_send())
@@ -364,11 +485,8 @@
     heads = lambdas.shape[0]
     cache_len = key_cache.shape[1]
     middle = HEAD_DIM // 2
-    inverse = ROPE_BASE ** (-jnp.arange(middle, dtype=F32) / middle)
-    angles = past_lengths.astype(F32)[:, None] * inverse[None, :]
-    cosine, sine = jnp.cos(angles), jnp.sin(angles)
-    cos = jnp.concatenate([cosine] * 4, axis=1)
-    sin = jnp.concatenate([-sine, sine] * 2, axis=1)
+    powers = ROPE_BASE ** (-np.arange(middle, dtype=np.float32) / np.float32(middle))
+    inverse = jnp.asarray(np.tile(powers.astype(np.float32), 128 // middle)[None, :])
     sem = pltpu.SemaphoreType.DMA
     part, key_new, value_new = pl.pallas_call(
         attention_kernel,
@@ -377,7 +495,7 @@
             jax.ShapeDtypeStruct((batch, 128), BF16),
             jax.ShapeDtypeStruct((batch, 128), BF16),
         ),
-        in_specs=[SMEM] + [VMEM] * 6 + [ANY] * 6,
+        in_specs=[SMEM] * 2 + [VMEM] * 5 + [ANY] * 6,
         out_specs=(VMEM, VMEM, VMEM),
         scratch_shapes=[
             pltpu.VMEM(w_query.shape, BF16),
@@ -395,27 +513,24 @@
         ],
         name="attend",
     )(
-        past_lengths, hidden_in, cos, sin, attn_gain.reshape(1, -1), lambdas.reshape(-1, 1),
-        head_gain.reshape(1, -1), w_query, w_key, w_value, w_out, key_cache, value_cache,
+        past_lengths, lambdas, past_lengths.reshape(1, -1), inverse, hidden_in,
+        attn_gain.reshape(1, -1), head_gain.reshape(1, -1), w_query, w_key, w_value, w_out, key_cache, value_cache,
     )
     experts = n_ep // 2
-    named = route_ids.T[None, :, :] == jnp.arange(experts)[:, None, None]
-    table = jnp.sum(jnp.where(named, route_weights.T[None, :, :], 0.0), axis=1)
-    table = jnp.pad(table, ((0, 0), (0, 128 - batch)))
     zs = 4 if n_ep % 4 == 0 else 1
     ms = n_ep // zs
     expert_w, dense_w = expert_gate.shape[2], dense_gate.shape[1]
     mixed = pl.pallas_call(
         functools.partial(ffn_kernel, n_ep, zs),
         out_shape=jax.ShapeDtypeStruct((batch, half), BF16),
-        in_specs=[VMEM] * 5 + [ANY] * 6,
+        in_specs=[VMEM] * 6 + [ANY] * 6,
         out_specs=VMEM,
         scratch_shapes=[
-            pltpu.VMEM(expert_gate.shape[1:], BF16),
-            pltpu.VMEM(expert_up.shape[1:], BF16),
+            pltpu.VMEM((expert_w, width), BF16),
+            pltpu.VMEM((expert_w, width), BF16),
             pltpu.VMEM(expert_down.shape[1:], BF16),
-            pltpu.VMEM(dense_gate.shape, BF16),
-            pltpu.VMEM(dense_up.shape, BF16),
+            pltpu.VMEM((dense_w, width), BF16),
+            pltpu.VMEM((dense_w, width), BF16),
             pltpu.VMEM(dense_down.shape, BF16),
             pltpu.VMEM((batch, width), BF16),
             pltpu.VMEM((batch, width), F32),
@@ -428,15 +543,16 @@
             pltpu.VMEM((zs, batch, half), BF16),
             pltpu.VMEM((zs, batch, half), BF16),
             pltpu.VMEM((batch, half), F32),
-            sem((6,)), sem((2,)), sem((n_ep,)), sem((n_ep,)), sem((zs,)), sem((zs, ms)), sem((n_ep,)),
+            sem((6,)), sem((2,)), sem((n_ep,)), sem((n_ep,)), sem((zs,)), sem((zs, ms)), sem((zs,)), sem((n_ep,)),
             sem((n_ep,)), sem((n_ep,)), sem((2, zs)), sem((2, zs)), sem((zs, ms)), sem((zs, ms)),
             sem((zs,)), sem((zs,)),
         ],
         compiler_params=pltpu.CompilerParams(collective_id=0, has_side_effects=True),
         name="feed",
     )(
-        part, hidden_in, ffn_gain.reshape(1, -1), table, gate_vector.astype(F32).reshape(1, -1),
-        expert_gate, expert_up, expert_down, dense_gate, dense_up, dense_down,
+        part, hidden_in, ffn_gain.reshape(1, -1), route_ids.T, route_weights.T, gate_vector.reshape(1, -1),
+        expert_gate.swapaxes(1, 2), expert_up.swapaxes(1, 2), expert_down,
+        dense_gate.T, dense_up.T, dense_down,
     )
     return mixed, key_new, value_new
 

time: 75.3 us -> 68.2 us (0.906)
  local copies, waits for them, and re-layouts: 9.13 us -> 2.76 us
  other arithmetic: 3.5 us -> 0 us
  Pallas kernels: 61.7 us -> 64.2 us
    unnamed x13 -> x1, local copies, waits for them, and re-layouts: 7.21 us -> 1.47 us
    pallas_call x1, Pallas kernels: 47.3 us -> 51 us  [per_device(): pl.pallas_call(functools.partial(ffn_kernel, n_ep, zs), out_shape=jax.Sha...]
    reshape x1 -> x0, other arithmetic: 1.28 us -> none  [per_device(): gate_vector.astype(F32).reshape(1, -1)]
    pallas_call x1, Pallas kernels: 14.4 us -> 13.1 us  [per_device(): pl.pallas_call(attention_kernel, out_shape=(jax.ShapeDtypeStruct((batch,...]
where the time goes in v2:
time: 68.2 us; the launch traced here: 67.6 us
  Pallas kernels  64.2 us (94%)
  local copies, waits for them, and re-layouts  2.76 us (4%)
    pallas_call x1, Pallas kernels, per_device(): pl.pallas_call(functools.partial(ffn_kernel, n_ep, zs), out_shape=jax.Sha...  51 us
    pallas_call x1, Pallas kernels, per_device(): pl.pallas_call(attention_kernel, out_shape=(jax.ShapeDtypeStruct((batch,...  13.1 us
    unnamed x1, local copies, waits for them, and re-layouts  1.47 us

profile of v2, /device:TPU:0, one launch (start us, length us, event | category | flops | bytes accessed | tf_op | source)
XLA Modules:
  0.0 67.6 jit_solution(15291408687079205205)
XLA Ops:
  0.6 1.3 %reshape.25.gvec = bf16[1,2048]{1,0:T(2,128)(2,1)} reshape(bf16[2048]{0:T(1024)(128)(2,1)} %param.39) | data formatting | bytes 8192 | tf_op jit(solution)/shard_map/reshape | solution.py:553
  1.9 13.1 %attend.1 = (bf16[32,2048]{1,0:T(8,128)(2,1)}, bf16[32,128]{1,0:T(8,128)(2,1)}, bf16[32,128]{1,0:T(8,128)(2,1)}) custom-call(s32[32]{0:T(128)} %lens.1, f32[8]{0:T(128)} %lam.1, s32[1,32]{1,0:T(1,128)} %bitcast.16, f32[1,128]{1,0:T(1,128)} %constant.2.clone.inverse, bf16[32,2048]{1,0:T(8,128)(2,1)} %hid.3, f32[1,2048]{1,0:T(1,128)} %bitcast.14, ...), custom_call_target="tpu_custom_call" | custom-call | tf_op jit(solution)/shard_map/attend/pallas_call | solution.py:491
  15.1 51.0 %feed.1 = bf16[32,1024]{1,0:T(8,128)(2,1)} custom-call(bf16[32,2048]{1,0:T(8,128)(2,1)} %get-tuple-element.6.part, bf16[32,2048]{1,0:T(8,128)(2,1)} %hid.3, f32[1,2048]{1,0:T(1,128)} %bitcast.15, s32[2,32]{1,0:T(2,128)} %bitcast.17, f32[2,32]{1,0:T(2,128)} %bitcast.18, bf16[1,2048]{1,0:T(2,128)(2,1)} %reshape.25.gvec, bf16[1,352,2048]{2,1,0:T(8,128)(2,1)} %bitcast.10, ...), custom_call_target="tpu_custom_call" | custom-call | tf_op jit(solution)/shard_map/feed/pallas_call | solution.py:523
  66.1 1.5 %copy.26 = bf16[32,1024]{1,0:T(8,128)(2,1)} copy(bf16[32,1024]{1,0:T(8,128)(2,1)} %feed.1) | data formatting | bytes 131072

commit v3 on v2

--- a/solution.py
+++ b/solution.py
@@ -162,7 +162,7 @@
     n, zs,
     part, hid, fgain, ids, shares, gvec, eg_any, eu_any, ed_any, dg_any, du_any, dd_any,
     out,
-    eg, eu, ed, dg, du, dd, peer, res, rows, wtb, eact, dact, sp, rp, zsend, zrecv, own,
+    eg, eu, ed, dg, du, dd, peer, res, rows, wtb, eact, dact, sp, rp, zsend, zrecv, own, gline,
     wsem, psem, rsend, rrecv, zs_send, pl_send, hop_send, arr, fw_send, fw_recv, as_send, as_recv,
     sp_send, rp_recv, zq_send, zq_recv,
 ):
@@ -185,6 +185,9 @@
         load.start()
 
     experts = wtb.shape[1]
+    gates = gvec[...].astype(F32)
+    gates = jnp.concatenate([gates[i:i + 1] for i in range(gates.shape[0])], axis=1)
+    gline[...] = gates
     numbers = lax.broadcasted_iota(jnp.int32, (experts, batch), 0)
     table = jnp.zeros((experts, batch), F32)
     for k in range(ids.shape[0]):
@@ -327,29 +330,6 @@
         acts(d, eact, 0).start()
         acts(d, dact, 1).start()
 
-    spread(0)
-
-    def gather_step(d):
-        @pl.when(d + 1 < zs)
-        def _():
-            spread(d + 1)
-
-        @pl.when(d < zs)
-        def _():
-            collect(d)
-
-        @pl.when(d == 1)
-        def _():
-            for load in loads:
-                load.wait()
-
-        @pl.when(d > 0)
-        def _():
-            first(d - 1)
-
-    loop(0, zs + 1, gather_step)
-    loop(1, n, lambda k: remote(
-        wtb.at[me], wtb.at[(me + k) % n], rsend.at[k], rrecv.at[(me + k) % n], other).wait_recv())
     expert = me // 2
 
     def send_part(zd, k):
@@ -373,20 +353,19 @@
         )
 
     def pass_on(i):
-        zd = (z + i + 1) % zs
+        zd = (z + i) % zs
         first_leg(zd, 0).wait_recv()
         rp[zd, 3] = (sp[zd, flip(p, far)].astype(F32) + rp[zd, 0].astype(F32)).astype(BF16)
         next_leg(zd).start()
 
     def second(i):
-        d = (i + 1) % zs
-        zd = (z + d) % zs
+        zd = (z + i) % zs
         for k, buf in enumerate((eact, dact)):
             remote(buf.at[1 - c, zd], buf.at[1 - c, zd], as_send.at[k, zd], as_recv.at[k, zd], other).wait_recv()
         block = pl.ds(zd * ms, ms)
         gate = (
-            jnp.sum(rows[0, block].reshape(ms * batch, half).astype(F32) * gvec[:, :half].astype(F32), axis=1, keepdims=True)
-            + jnp.sum(rows[1, block].reshape(ms * batch, half).astype(F32) * gvec[:, half:].astype(F32), axis=1, keepdims=True)
+            jnp.sum(rows[0, block].reshape(ms * batch, half).astype(F32) * gline[:, :half], axis=1, keepdims=True)
+            + jnp.sum(rows[1, block].reshape(ms * batch, half).astype(F32) * gline[:, half:], axis=1, keepdims=True)
         )
         gate = (1.0 / (1.0 + jnp.exp(-gate))).astype(BF16).astype(F32)
         share = jnp.concatenate([
@@ -427,21 +406,28 @@
         zsend[zd] = gathered(zd).astype(BF16)
         zback(d).start()
 
-    def reduce_step(i):
-        @pl.when(i < zs)
-        def _():
-            second(i)
-
-        if quad:
-            @pl.when((i > 0) & (i <= zs))
-            def _():
-                pass_on(i - 1)
-
-        @pl.when((i > 1) & (i <= zs))
-        def _():
-            third(i - 1)
-
-    loop(0, zs + 1, reduce_step)
+    def stage(low, high, t, body):
+        pl.when((t >= low) & (t < high))(body)
+
+    def route_arrivals():
+        for load in loads:
+            load.wait()
+        loop(1, n, lambda k: remote(
+            wtb.at[me], wtb.at[(me + k) % n], rsend.at[k], rrecv.at[(me + k) % n], other).wait_recv())
+
+    spread(0)
+
+    def step(t):
+        stage(0, zs - 1, t, lambda: spread(t + 1))
+        stage(0, zs, t, lambda: collect(t))
+        stage(1, 2, t, route_arrivals)
+        stage(1, zs + 1, t, lambda: first(t - 1))
+        stage(2, zs + 2, t, lambda: second(t - 2))
+        if quad:
+            stage(3, zs + 3, t, lambda: pass_on(t - 3))
+        stage(5, zs + 4, t, lambda: third(t - 4))
+
+    loop(0, zs + 4, step)
     own[...] = gathered(z) + res[:, pl.ds(pl.multiple_of(c * half, half), half)]
 
     def last(d):
@@ -543,6 +529,7 @@
             pltpu.VMEM((zs, batch, half), BF16),
             pltpu.VMEM((zs, batch, half), BF16),
             pltpu.VMEM((batch, half), F32),
+            pltpu.VMEM((1, width), F32),
             sem((6,)), sem((2,)), sem((n_ep,)), sem((n_ep,)), sem((zs,)), sem((zs, ms)), sem((zs,)), sem((n_ep,)),
             sem((n_ep,)), sem((n_ep,)), sem((2, zs)), sem((2, zs)), sem((zs, ms)), sem((zs, ms)),
             sem((zs,)), sem((zs,)),
@@ -550,7 +537,7 @@
         compiler_params=pltpu.CompilerParams(collective_id=0, has_side_effects=True),
         name="feed",
     )(
-        part, hidden_in, ffn_gain.reshape(1, -1), route_ids.T, route_weights.T, gate_vector.reshape(1, -1),
+        part, hidden_in, ffn_gain.reshape(1, -1), route_ids.T, route_weights.T, gate_vector.reshape(-1, 128),
         expert_gate.swapaxes(1, 2), expert_up.swapaxes(1, 2), expert_down,
         dense_gate.T, dense_up.T, dense_down,
     )

time: 68.2 us -> 64.7 us (0.949)
  Pallas kernels: 64.2 us -> 62.1 us
  local copies, waits for them, and re-layouts: 2.76 us -> 1.47 us
    pallas_call x1, Pallas kernels: 51 us -> 48.8 us  [per_device(): pl.pallas_call(functools.partial(ffn_kernel, n_ep, zs), out_shape=jax.Sha...]
    reshape x1 -> x0, local copies, waits for them, and re-layouts: 1.29 us -> none  [per_device(): gate_vector.reshape(1, -1)]
where the time goes in v3:
time: 64.7 us; the launch traced here: 64.2 us
  Pallas kernels  62.1 us (96%)
  local copies, waits for them, and re-layouts  1.47 us (2%)
  between operations  0.65 us (1%)
    pallas_call x1, Pallas kernels, per_device(): pl.pallas_call(functools.partial(ffn_kernel, n_ep, zs), out_shape=jax.Sha...  48.8 us
    pallas_call x1, Pallas kernels, per_device(): pl.pallas_call(attention_kernel, out_shape=(jax.ShapeDtypeStruct((batch,...  13.3 us
    unnamed x1, local copies, waits for them, and re-layouts  1.47 us

profile of v3, /device:TPU:0, one launch (start us, length us, event | category | flops | bytes accessed | tf_op | source)
XLA Modules:
  0.0 64.2 jit_solution(1169245530026634766)
XLA Ops:
  0.6 13.3 %attend.1 = (bf16[32,2048]{1,0:T(8,128)(2,1)}, bf16[32,128]{1,0:T(8,128)(2,1)}, bf16[32,128]{1,0:T(8,128)(2,1)}) custom-call(s32[32]{0:T(128)} %lens.1, f32[8]{0:T(128)} %lam.1, s32[1,32]{1,0:T(1,128)} %bitcast.18, f32[1,128]{1,0:T(1,128)} %constant.2.clone.inverse, bf16[32,2048]{1,0:T(8,128)(2,1)} %hid.3, f32[1,2048]{1,0:T(1,128)} %bitcast.15, ...), custom_call_target="tpu_custom_call" | custom-call | tf_op jit(solution)/shard_map/attend/pallas_call | solution.py:477
  14.0 48.8 %feed.1 = bf16[32,1024]{1,0:T(8,128)(2,1)} custom-call(bf16[32,2048]{1,0:T(8,128)(2,1)} %get-tuple-element.6.part, bf16[32,2048]{1,0:T(8,128)(2,1)} %hid.3, f32[1,2048]{1,0:T(1,128)} %bitcast.16, s32[2,32]{1,0:T(2,128)} %bitcast.19, f32[2,32]{1,0:T(2,128)} %bitcast.20, bf16[16,128]{1,0:T(8,128)(2,1)} %bitcast.17, bf16[1,352,2048]{2,1,0:T(8,128)(2,1)} %bitcast.11, ...), custom_call_target="tpu_custom_call" | custom-call | tf_op jit(solution)/shard_map/feed/pallas_call | solution.py:509
  62.8 1.5 %copy.26 = bf16[32,1024]{1,0:T(8,128)(2,1)} copy(bf16[32,1024]{1,0:T(8,128)(2,1)} %feed.1) | data formatting | bytes 131072
